TPU v7x, 256 devices: a whole 4x4x8 slice. The times are simulated.
256 devices in a mesh: sp: 16 (over y, x), tp: 16 (over z, core).
Axes of the slice: x: 4, y: 4, z: 8, core: 2. Of those that a mesh axis runs over, the one named last changes fastest.
Arguments:
- upstream: bfloat16 [4096, 4096], P('sp', 'tp'), may hold values from -6 to 6
- stream: bfloat16 [4096, 4096], P('sp', 'tp'), may hold values from -400 to 400
- norm_gain: float32 [4096], P('tp'), may hold values from 0.1 to 1.9
- routes: int32 [4096, 2], P('sp'), may hold values from 0 to 15, all different within a row; in each aligned block of 256 rows (0 to 255, 256 to 511, ...) at most 48 rows name the same one
- route_weights: float32 [4096, 2], P('sp'), may hold values from 0.1 to 1
- w_gate: bfloat16 [16, 4096, 2048], P('sp', None, 'tp'), may hold values from -0.09375 to 0.09375
- w_up: bfloat16 [16, 4096, 2048], P('sp', None, 'tp'), may hold values from -0.09375 to 0.09375
- w_down: bfloat16 [16, 2048, 4096], P('sp', 'tp'), may hold values from -0.125 to 0.125
- value_in: bfloat16 [4096, 2048], P('sp', 'tp'), may hold values from -6 to 6
- gate_in: bfloat16 [4096, 2048], P('sp', 'tp'), may hold values from -6 to 6
- conv_pre: bfloat16 [4096, 2048], P('sp', 'tp'), may hold values from -200 to 200
- ln_gain: float32 [2048], P('tp'), may hold values from 0.1 to 1.9
- conv_taps: float32 [31, 2048], P(None, 'tp'), may hold values from -1 to 1
- w_out: bfloat16 [2048, 4096], P('tp'), may hold values from -0.125 to 0.125
Outputs:
- grad_gate: float32 [16, 4096, 2048], P('sp', None, 'tp')
- grad_up: float32 [16, 4096, 2048], P('sp', None, 'tp')
- grad_down: float32 [16, 2048, 4096], P('sp', 'tp')
- grad_out: float32 [2048, 4096], P('tp', 'sp')
- value_grad: bfloat16 [4096, 2048], P('sp', 'tp')
- gate_grad: bfloat16 [4096, 2048], P('sp', 'tp')
Inputs may be any that keep to these rules, and one draw needn't show every extreme that they name: `routes`: each token names two different experts. Among the tokens of one index of sp no expert is named more than 48 times, and in every draw some expert exactly 48 times.
All inputs are finite; a program needn't handle non-finite values.
Results may differ from a plain program's by a relative error of at most 0.0071.
Values may be sent and summed in bfloat16 or wider, within the bound.
No kernel may reach another device: no remote copies, remote signals or barrier semaphores. Data moves between devices by JAX's collectives and lax.ppermute only.
A program may use at most 128 MiB of HBM per device.

v0:
```python
import jax
import jax.numpy as jnp
from jax import lax
from jax.sharding import PartitionSpec as P

EPSILON = 1e-06


def sent_to_all(value, axis):
    count = lax.axis_size(axis)
    return lax.all_to_all(
        jnp.broadcast_to(value[None], (count, *value.shape)), axis, 0, 0, tiled=True
    )


def of_everyone(value, axis):
    everything = sent_to_all(value, axis)
    return jnp.sum(everything, axis=0)


def in_one(arrays, axis):
    vector, at, gathered = (jnp.concatenate([a.reshape(-1) for a in arrays]), 0, [])
    total = of_everyone(vector, axis)
    for a in arrays:
        gathered.append(total[at : at + a.size].reshape(a.shape))
        at += a.size
    return tuple(gathered)


def side_by_side(arrays, axis, split_dim, concat_dim, along):
    both = jnp.concatenate(arrays, axis=along)
    out, at, gathered = (
        lax.all_to_all(both, axis, split_axis=split_dim, concat_axis=concat_dim, tiled=True),
        0,
        [],
    )
    for a in arrays:
        gathered.append(lax.slice_in_dim(out, at, at + a.shape[along], axis=along))
        at += a.shape[along]
    return tuple(gathered)


def in_one_piece(arrays, axis, dim, along):
    widths = [a.shape[along] for a in arrays]
    both = jnp.concatenate(arrays, axis=along)
    out = lax.all_gather(both, axis, axis=dim, tiled=True)
    return tuple(jnp.split(out, [sum(widths[:k]) for k in range(1, len(widths))], axis=along))


def cut_along(value, dim, count):
    shape = value.shape
    blocks = value.reshape(*shape[:dim], count, shape[dim] // count, *shape[dim + 1 :])
    return jnp.moveaxis(blocks, dim, 0)


def sent_and_summed(value, axis, dim):
    count = lax.axis_size(axis)
    blocks = lax.all_to_all(cut_along(value, dim, count), axis, 0, 0, tiled=True)
    return jnp.sum(blocks.astype(jnp.float32), axis=0)


def shifted(block, axis, distance):
    devices = range(lax.axis_size(axis))
    route = [(i - distance, i) for i in devices if i - distance in devices]
    return lax.ppermute(block, axis, route)


def silu_slope(values):
    logistic = jax.nn.sigmoid(values)
    return logistic * (1.0 + values * (1.0 - logistic))


def per_device(
    upstream,
    stream,
    norm_gain,
    routes,
    route_weights,
    w_gate,
    w_up,
    w_down,
    value_in,
    gate_in,
    conv_pre,
    ln_gain,
    conv_taps,
    w_out,
):
    tok_rows, width_part = stream.shape
    token_groups = lax.axis_size("sp")
    width_groups = lax.axis_size("tp")
    model_width = width_part * width_groups
    channels = conv_pre.shape[1] * width_groups
    tap_count = conv_taps.shape[0]
    capacity = 3 * tok_rows // token_groups
    experts = w_gate.shape[0] * token_groups
    slot_count = experts * capacity
    expert_rows = token_groups * capacity
    residual = stream.astype(jnp.float32)
    conv_vals = conv_pre.astype(jnp.float32)
    row_squares, conv_total, conv_squares = in_one(
        (
            jnp.sum(residual * residual, axis=1),
            jnp.sum(conv_vals, axis=1),
            jnp.sum(conv_vals * conv_vals, axis=1),
        ),
        "tp",
    )
    inverse = lax.rsqrt(row_squares / model_width + EPSILON)[:, None]
    normed = (norm_gain[None, :] * residual * inverse).astype(jnp.bfloat16)
    flat_experts = routes.reshape(-1)
    one_hot = (flat_experts[:, None] == jnp.arange(experts, dtype=jnp.int32)[None, :]).astype(
        jnp.int32
    )
    slot_rank = jnp.sum((jnp.cumsum(one_hot, axis=0) - one_hot) * one_hot, axis=1)
    slot_index = (flat_experts * capacity + slot_rank).reshape(tok_rows, 2)
    slot_ids = jnp.arange(slot_count, dtype=jnp.int32)[:, None]
    first_hit = slot_ids == slot_index[None, :, 0]
    second_hit = slot_ids == slot_index[None, :, 1]
    any_hit = jnp.logical_or(first_hit, second_hit)
    picker = any_hit.astype(jnp.bfloat16)
    slot_weight = jnp.sum(
        jnp.where(first_hit, route_weights[None, :, 0], 0.0)
        + jnp.where(second_hit, route_weights[None, :, 1], 0.0),
        axis=1,
    )
    token_iota = jnp.arange(tok_rows, dtype=jnp.int32)[None, :]
    slot_token = jnp.where(
        jnp.any(any_hit, axis=1), jnp.sum(jnp.where(any_hit, token_iota, 0), axis=1), tok_rows
    )
    columns = normed.shape[1]
    normed_pad = jnp.concatenate([normed, jnp.zeros((1, columns), jnp.bfloat16)], axis=0)
    upstream_pad = jnp.concatenate([upstream, jnp.zeros((1, columns), jnp.bfloat16)], axis=0)
    inputs = normed_pad[slot_token]
    cotangent = (upstream_pad[slot_token].astype(jnp.float32) * slot_weight[:, None]).astype(
        jnp.bfloat16
    )
    sent_inputs = inputs.reshape(experts, capacity, columns)
    sent_cotangent = cotangent.reshape(experts, capacity, columns)
    part_inputs, part_cotangent = side_by_side((sent_inputs, sent_cotangent), "sp", 0, 0, 1)
    inputs, cotangent = in_one_piece(
        (
            part_inputs.reshape(expert_rows, width_part),
            part_cotangent.reshape(expert_rows, width_part),
        ),
        "tp",
        1,
        0,
    )
    gate_mat = w_gate[0]
    upper_mat = w_up[0]
    down_mat = w_down[0]
    gate_pre = jnp.dot(inputs, gate_mat, preferred_element_type=jnp.float32)
    upper_pre = jnp.dot(inputs, upper_mat, preferred_element_type=jnp.float32)
    active = (jax.nn.silu(gate_pre) * upper_pre).astype(jnp.bfloat16)
    active_back = lax.dot_general(
        cotangent, down_mat, (((1,), (1,)), ((), ())), preferred_element_type=jnp.float32
    )
    gate_back = (active_back * upper_pre * silu_slope(gate_pre)).astype(jnp.bfloat16)
    upper_back = (active_back * jax.nn.silu(gate_pre)).astype(jnp.bfloat16)
    grad_gate = lax.dot_general(
        inputs, gate_back, (((0,), (0,)), ((), ())), preferred_element_type=jnp.float32
    )
    grad_up = lax.dot_general(
        inputs, upper_back, (((0,), (0,)), ((), ())), preferred_element_type=jnp.float32
    )
    grad_down = lax.dot_general(
        active, cotangent, (((0,), (0,)), ((), ())), preferred_element_type=jnp.float32
    )
    input_part = lax.dot_general(
        gate_back, gate_mat, (((1,), (1,)), ((), ())), preferred_element_type=jnp.float32
    ) + lax.dot_general(
        upper_back, upper_mat, (((1,), (1,)), ((), ())), preferred_element_type=jnp.float32
    )
    input_back = lax.psum_scatter(
        input_part.astype(jnp.bfloat16), "tp", scatter_dimension=1, tiled=True
    )
    returned = lax.all_to_all(
        input_back.reshape(token_groups, capacity, width_part),
        "sp",
        split_axis=0,
        concat_axis=0,
        tiled=True,
    )
    returned = returned.reshape(slot_count, width_part)
    token_back = lax.dot_general(
        picker, returned, (((0,), (0,)), ((), ())), preferred_element_type=jnp.float32
    )
    gained = norm_gain[None, :] * token_back
    inner_sum = of_everyone(jnp.sum(gained * residual, axis=1), "tp")
    norm_back = inverse * gained - residual * inverse**3 * (inner_sum / model_width)[:, None]
    stream_grad = (upstream.astype(jnp.float32) + norm_back).astype(jnp.bfloat16)
    full_grad = lax.all_gather(stream_grad, "tp", axis=1, tiled=True)
    mean_val = (conv_total / channels)[:, None]
    variance = (conv_squares / channels)[:, None] - mean_val * mean_val
    inv_std = lax.rsqrt(variance + EPSILON)
    centred = (conv_vals - mean_val) * inv_std
    scaled = centred * ln_gain[None, :]
    mixed_out = jax.nn.silu(scaled).astype(jnp.bfloat16)
    columns = full_grad
    grad_rows = sent_and_summed(
        lax.dot_general(
            columns, mixed_out, (((0,), (0,)), ((), ())), preferred_element_type=jnp.float32
        ).astype(jnp.bfloat16),
        "sp",
        0,
    )
    grad_out = grad_rows.T
    mixed_back = lax.dot_general(
        full_grad, w_out, (((1,), (1,)), ((), ())), preferred_element_type=jnp.float32
    )
    norm_in = mixed_back * silu_slope(scaled) * ln_gain[None, :]
    norm_total, norm_cross = in_one(
        (jnp.sum(norm_in, axis=1), jnp.sum(norm_in * centred, axis=1)), "tp"
    )
    conv_back = inv_std * (
        norm_in - (norm_total / channels)[:, None] - centred * (norm_cross / channels)[:, None]
    )
    next_rim = shifted(conv_back[: tap_count - 1], "sp", -1)
    padded = jnp.concatenate([conv_back, next_rim], axis=0)
    glu_back = jnp.zeros(conv_back.shape, jnp.float32)
    for tap_index in range(tap_count):
        offset = tap_count - 1 - tap_index
        glu_back = glu_back + conv_taps[tap_index][None, :] * padded[offset : offset + tok_rows]
    gate_sigma = jax.nn.sigmoid(gate_in.astype(jnp.float32))
    value_grad = (glu_back * gate_sigma).astype(jnp.bfloat16)
    gate_grad = (glu_back * value_in.astype(jnp.float32) * gate_sigma * (1.0 - gate_sigma)).astype(
        jnp.bfloat16
    )
    return (grad_gate[None], grad_up[None], grad_down[None], grad_out, value_grad, gate_grad)


def solution(mesh):
    return jax.shard_map(
        per_device,
        mesh=mesh,
        in_specs=(
            P("sp", "tp"),
            P("sp", "tp"),
            P("tp"),
            P("sp", None),
            P("sp", None),
            P("sp", None, "tp"),
            P("sp", None, "tp"),
            P("sp", "tp", None),
            P("sp", "tp"),
            P("sp", "tp"),
            P("sp", "tp"),
            P("tp"),
            P(None, "tp"),
            P("tp", None),
        ),
        out_specs=(
            P("sp", None, "tp"),
            P("sp", None, "tp"),
            P("sp", "tp", None),
            P("tp", "sp"),
            P("sp", "tp"),
            P("sp", "tp"),
        ),
        check_vma=False,
    )
```

profile of v0, /device:TPU:1, one launch (start us, length us, event | category | flops | bytes accessed | tf_op | source)
XLA Modules:
  0.0 325.8 jit_solution(10947476030596708137)
XLA Ops:
  7.2 1.1 copy.69
  8.3 1.0 convert_reduce_fusion.1
  9.3 0.6 broadcast_in_dim.81
  10.0 10.0 %all-to-all-start = ((f32[16,1,768]{2,1,0:T(1,128)}), f32[16,1,768]{2,1,0:T(1,128)S(1)}, u32[]{:S(2)}, u32[]{:S(2)}) async-start(f32[16,1,768]{2,1,0:T(1,128)} %broadcast_in_dim.81), calls=%async_computation | async-start | bytes 98304 | tf_op jit(solution)/shard_map/all_to_all | solution.py:11
  20.0 0.8 copy.71
  20.8 0.1 eq.56
  21.0 0.1 eq.60
  21.1 1.2 reduce-window.6
  22.3 0.2 slice_reduce_fusion
  22.5 0.1 fusion.149
  22.6 0.1 reduce_sum.124
  22.8 0.1 copy.74
  22.9 0.7 multiply_add_fusion
  23.6 0.2 fusion.23
  23.8 0.2 select_reduce_fusion
  24.0 0.8 fusion.157
  24.8 0.2 add_reduce_fusion
  25.0 0.1 mul.484
  25.1 0.9 concatenate.23
  26.0 2.7 gather_fusion.1
  28.7 0.2 fusion.20
  28.9 0.6 slice_multiply_fusion.2
  29.5 0.8 fusion.28
  30.3 0.1 copy.88
  30.5 2.7 gather_fusion
  33.1 0.1 pad_maximum_fusion
  33.2 20.6 %all_to_all.33 = bf16[16,96,256]{2,1,0:T(8,128)(2,1)S(1)} all-to-all(bf16[16,96,256]{2,1,0:T(8,128)(2,1)S(1)} %pad_maximum_fusion), channel_id=1, replica_groups=mesh['sp'=16,'tp'=16] {'sp'}, dimensions={0} | all-to-all | bytes 1572864 | tf_op jit(solution)/shard_map/all_to_all | solution.py:33
  53.9 0.9 pad_maximum_fusion.1
  54.8 0.2 reduce-scatter.2.cloned.1.call-start
  55.1 79.9 %all-gather.3.cloned.1.call-done = bf16[1536,4096]{1,0:T(8,128)(2,1)} async-done(((bf16[1536,256]{1,0:T(8,128)(2,1)}), bf16[1536,4096]{1,0:T(8,128)(2,1)}) %all-gather.3.cloned.1.call-update) | async-done | bytes 12582928 | tf_op jit(solution)/shard_map/all_gather | solution.py:46
  134.9 4.7 %fusion.9 = f32[768,128]{1,0:T(8,128)S(1)} fusion(bf16[1536,4096]{1,0:T(8,128)(2,1)} %all-gather.3.cloned.1.call-done, bf16[1,4096,128]{2,1,0:T(8,128)(2,1)S(1)} %copy-done), kind=kOutput, calls=%fused_computation.13 | convolution fusion | flops 805306368 | bytes 7733248 | tf_op jit(solution)/shard_map/dot_general | solution.py:153
  139.7 5.2 %fusion.11 = f32[768,128]{1,0:T(8,128)S(1)} fusion(bf16[1536,4096]{1,0:T(8,128)(2,1)} %all-gather.3.cloned.1.call-done, bf16[1,4096,128]{2,1,0:T(8,128)(2,1)S(1)} %copy-done.2), kind=kOutput, calls=%fused_computation.15 | convolution fusion | flops 805306368 | bytes 7733248 | tf_op jit(solution)/shard_map/dot_general | solution.py:154
  144.9 1.8 multiply_convert_fusion.1
  146.7 1.8 fusion.14
  148.5 4.4 %add_convert_fusion = bf16[768,4096]{1,0:T(8,128)(2,1)} fusion(f32[768,4096]{1,0:T(8,128)S(1)} %fusion.14, bf16[768,128]{1,0:T(8,128)(2,1)S(1)} %get-tuple-element.36, bf16[1,4096,128]{2,1,0:T(8,128)(2,1)S(1)} %copy-done.2), kind=kOutput, calls=%fused_computation.2 | convolution fusion | flops 811597824 | bytes 20119552 | tf_op jit(solution)/shard_map/dot_general | solution.py:172
  153.0 61.9 %reduce-scatter.2.cloned.1.call-done = bf16[768,256]{1,0:T(8,128)(2,1)} async-done(((bf16[768,4096]{1,0:T(8,128)(2,1)}), bf16[768,256]{1,0:T(8,128)(2,1)}) %reduce-scatter.2.cloned.1.call-update) | async-done | bytes 393232 | tf_op jit(solution)/shard_map/reduce_scatter | solution.py:175
  214.8 14.7 %all_to_all.34 = bf16[16,48,256]{2,1,0:T(8,128)(2,1)S(1)} all-to-all(bf16[16,48,256]{2,1,0:T(8,128)(2,1)} %bitcast.128), channel_id=1, replica_groups=mesh['sp'=16,'tp'=16] {'sp'}, dimensions={0} | all-to-all | bytes 786432 | tf_op jit(solution)/shard_map/all_to_all | solution.py:178
  229.6 0.4 fusion.34
  230.0 0.6 broadcast_in_dim.93
  230.6 9.6 %all-to-all-start.3 = ((f32[16,1,256]{2,1,0:T(1,128)}), f32[16,1,256]{2,1,0:T(1,128)S(1)}, u32[]{:S(2)}, u32[]{:S(2)}) async-start(f32[16,1,256]{2,1,0:T(1,128)} %broadcast_in_dim.93), calls=%async_computation.4 | async-start | bytes 32768 | tf_op jit(solution)/shard_map/all_to_all | solution.py:11
  240.2 0.3 all-gather.5.cloned.1.call-start
  240.5 0.1 copy.76
  240.6 7.0 %all-to-all-done.3 = f32[16,1,256]{2,1,0:T(1,128)S(1)} async-done(((f32[16,1,256]{2,1,0:T(1,128)}), f32[16,1,256]{2,1,0:T(1,128)S(1)}, u32[]{:S(2)}, u32[]{:S(2)}) %all-to-all-start.3) | async-done | bytes 16416 | tf_op jit(solution)/shard_map/all_to_all | solution.py:11
  247.6 0.7 fusion.33
  248.4 0.5 slice_bitcast_fusion.29
  248.9 0.7 slice_bitcast_fusion.30
  249.6 5.9 %convolution_bitcast_fusion.1 = f32[1,4096,128]{2,1,0:T(8,128)} fusion(bf16[768,128]{1,0:T(8,128)(2,1)S(1)} %get-tuple-element.37, bf16[1536,4096]{1,0:T(8,128)(2,1)} %all-gather.3.cloned.1.call-done), kind=kOutput, calls=%fused_computation.9 | convolution fusion | flops 805306368 | bytes 8585216 | tf_op jit(solution)/shard_map/dot_general | solution.py:161
  255.5 6.1 %convolution_bitcast_fusion = f32[1,4096,128]{2,1,0:T(8,128)} fusion(bf16[768,128]{1,0:T(8,128)(2,1)S(1)} %get-tuple-element.36, bf16[1536,4096]{1,0:T(8,128)(2,1)} %all-gather.3.cloned.1.call-done), kind=kOutput, calls=%fused_computation.8 | convolution fusion | flops 805306368 | bytes 8585216 | tf_op jit(solution)/shard_map/dot_general | solution.py:164
  261.7 18.9 %all-gather.5.cloned.1.call-done = bf16[256,4096]{0,1:T(8,128)(2,1)} async-done(((bf16[256,256]{0,1:T(8,128)(2,1)}), bf16[256,4096]{0,1:T(8,128)(2,1)}) %all-gather.5.cloned.1.call-update) | async-done | bytes 2097168 | tf_op jit(solution)/shard_map/all_gather | solution.py:193
  280.6 2.5 fusion.154
  283.1 0.6 broadcast_in_dim.94
  283.7 4.4 %all-to-all-start.5 = ((f32[16,1,512]{2,1,0:T(1,128)}), f32[16,1,512]{2,1,0:T(1,128)S(1)}, u32[]{:S(2)}, u32[]{:S(2)}) async-start(f32[16,1,512]{2,1,0:T(1,128)} %broadcast_in_dim.94), calls=%async_computation.6 | async-start | bytes 65536 | tf_op jit(solution)/shard_map/all_to_all | solution.py:11
  288.1 3.4 %convolution_convert_fusion = bf16[4096,128]{1,0:T(8,128)(2,1)} fusion(bf16[256,4096]{0,1:T(8,128)(2,1)} %all-gather.5.cloned.1.call-done, bf16[256,128]{1,0:T(8,128)(2,1)S(1)} %copy-done.3, f32[128]{0:T(128)S(1)} %copy-done.36, f32[256]{0:T(256)S(1)} %copy-done.9, f32[256]{0:T(256)S(1)} %copy-done.8), kind=kOutput, calls=%fused_computation.10 | convolution fusion | flops 269254656 | bytes 3213824 | tf_op jit(solution)/shard_map/dot_general | solution.py:202
  291.7 3.8 %all-to-all-done.5 = f32[16,1,512]{2,1,0:T(1,128)S(1)} async-done(((f32[16,1,512]{2,1,0:T(1,128)}), f32[16,1,512]{2,1,0:T(1,128)S(1)}, u32[]{:S(2)}, u32[]{:S(2)}) %all-to-all-start.5) | async-done | bytes 32800 | tf_op jit(solution)/shard_map/all_to_all | solution.py:11
  295.5 6.5 %all-to-all-start.4 = ((bf16[16,256,128]{2,1,0:T(8,128)(2,1)}), bf16[16,256,128]{2,1,0:T(8,128)(2,1)S(1)}, u32[]{:S(2)}, u32[]{:S(2)}) async-start(bf16[16,256,128]{2,1,0:T(8,128)(2,1)} %bitcast.17), calls=%async_computation.5 | async-start | bytes 2097152 | tf_op jit(solution)/shard_map/all_to_all | solution.py:58
  302.1 0.2 fusion.139
  302.3 1.3 collective-permute-start
  303.6 5.2 %fusion.4 = f32[1,128,4096]{2,1,0:T(8,128)} fusion(bf16[1536,4096]{1,0:T(8,128)(2,1)} %all-gather.3.cloned.1.call-done, f32[768,128]{1,0:T(8,128)S(1)} %fusion.11, f32[768,128]{1,0:T(8,128)S(1)} %fusion.9), kind=kOutput, calls=%fused_computation.7 | convolution fusion | flops 805896192 | bytes 9175040 | tf_op jit(solution)/shard_map/dot_general | solution.py:167
  308.8 6.6 %collective-permute-done = f32[30,128]{1,0:T(8,128)S(1)} collective-permute-done((f32[30,128]{1,0:T(8,128)S(1)}, f32[30,128]{1,0:T(8,128)S(1)}, u32[]{:S(2)}, u32[]{:S(2)}) %collective-permute-start) | collective-permute-done | bytes 15392 | tf_op jit(solution)/shard_map/ppermute | solution.py:65
  315.6 1.1 multiply_convert_fusion.4
  316.8 0.7 multiply_convert_fusion.5
  317.5 0.9 all-to-all-done.4
  318.4 0.1 convert_reduce_fusion
  318.5 0.8 copy.79
  (101 shorter events, 0.6 us)
Async XLA Ops:
  7.2 127.7 %copy-start = (bf16[1,4096,128]{2,1,0:T(8,128)(2,1)S(1)}, bf16[1,4096,128]{2,1,0:T(8,128)(2,1)}, u32[]{:S(2)}) copy-start(bf16[1,4096,128]{2,1,0:T(8,128)(2,1)} %param.19) | copy-start | bytes 3145732
  10.0 18.9 %all-to-all-start = ((f32[16,1,768]{2,1,0:T(1,128)}), f32[16,1,768]{2,1,0:T(1,128)S(1)}, u32[]{:S(2)}, u32[]{:S(2)}) async-start(f32[16,1,768]{2,1,0:T(1,128)} %broadcast_in_dim.81), calls=%async_computation | async-start | bytes 98304 | tf_op jit(solution)/shard_map/all_to_all | solution.py:11
  20.0 115.0 %all-gather.3.cloned.1.call-start = ((), (), s32[]{:S(2)}) async-start(), calls=%async_computation.7 | async-start | bytes 13369344 | tf_op jit(solution)/shard_map/all_gather | solution.py:46
  53.9 85.8 %copy-start.2 = (bf16[1,4096,128]{2,1,0:T(8,128)(2,1)S(1)}, bf16[1,4096,128]{2,1,0:T(8,128)(2,1)}, u32[]{:S(2)}) copy-start(bf16[1,4096,128]{2,1,0:T(8,128)(2,1)} %param.20) | copy-start | bytes 3145732
  54.8 160.0 %reduce-scatter.2.cloned.1.call-start = ((), (), s32[]{:S(2)}) async-start(), calls=%async_computation.8 | async-start | bytes 6684672 | tf_op jit(solution)/shard_map/reduce_scatter | solution.py:175
  134.9 10.0 %copy-start.1 = (bf16[1536,4096]{1,0:T(8,128)(2,1)S(1)}, bf16[1536,4096]{1,0:T(8,128)(2,1)}, u32[]{:S(2)}) copy-start(bf16[1536,4096]{1,0:T(8,128)(2,1)} %all-gather.3.cloned.1.call-done) | copy-start | bytes 37748740
  139.6 5.3 %copy-start.37 = (bf16[1,128,4096]{2,1,0:T(8,128)(2,1)S(1)}, bf16[1,128,4096]{2,1,0:T(8,128)(2,1)}, u32[]{:S(2)}) copy-start(bf16[1,128,4096]{2,1,0:T(8,128)(2,1)} %param.21) | copy-start | bytes 3145732
  153.0 76.6 %copy-start.35 = (f32[256]{0:T(256)S(1)}, f32[256]{0:T(256)}, u32[]{:S(2)}) copy-start(f32[256]{0:T(256)} %param.16) | copy-start | bytes 3076
  153.0 87.5 %copy-start.4 = (bf16[256,256]{1,0:T(8,128)(2,1)S(1)}, bf16[256,256]{1,0:T(8,128)(2,1)}, u32[]{:S(2)}) copy-start(bf16[256,256]{1,0:T(8,128)(2,1)} %param.14) | copy-start | bytes 393220
  153.0 94.6 %copy-start.10 = (f32[256]{0:T(256)S(1)}, f32[256]{0:T(256)}, u32[]{:S(2)}) copy-start(f32[256]{0:T(256)} %get-tuple-element.72) | copy-start | bytes 3076
  153.0 95.4 %copy-start.7 = (f32[31,128]{1,0:T(8,128)S(1)}, f32[31,128]{1,0:T(8,128)}, u32[]{:S(2)}) copy-start(f32[31,128]{1,0:T(8,128)} %param.26) | copy-start | bytes 47620
  230.6 16.9 %all-to-all-start.3 = ((f32[16,1,256]{2,1,0:T(1,128)}), f32[16,1,256]{2,1,0:T(1,128)S(1)}, u32[]{:S(2)}, u32[]{:S(2)}) async-start(f32[16,1,256]{2,1,0:T(1,128)} %broadcast_in_dim.93), calls=%async_computation.4 | async-start | bytes 32768 | tf_op jit(solution)/shard_map/all_to_all | solution.py:11
  240.2 40.4 %all-gather.5.cloned.1.call-start = ((), (), s32[]{:S(2)}) async-start(), calls=%async_computation.9 | async-start | bytes 2228224 | tf_op jit(solution)/shard_map/all_gather | solution.py:193
  255.5 25.1 %copy-start.3 = (bf16[256,128]{1,0:T(8,128)(2,1)S(1)}, bf16[256,128]{1,0:T(8,128)(2,1)}, u32[]{:S(2)}) copy-start(bf16[256,128]{1,0:T(8,128)(2,1)} %param.24) | copy-start | bytes 196612
  255.5 25.1 %copy-start.8 = (f32[256]{0:T(256)S(1)}, f32[256]{0:T(256)}, u32[]{:S(2)}) copy-start(f32[256]{0:T(256)} %get-tuple-element.71) | copy-start | bytes 3076
  255.5 25.1 %copy-start.9 = (f32[256]{0:T(256)S(1)}, f32[256]{0:T(256)}, u32[]{:S(2)}) copy-start(f32[256]{0:T(256)} %get-tuple-element.74) | copy-start | bytes 3076
  255.5 25.1 %copy-start.36 = (f32[128]{0:T(128)S(1)}, f32[128]{0:T(128)}, u32[]{:S(2)}) copy-start(f32[128]{0:T(128)} %param.25) | copy-start | bytes 1540
  255.5 25.1 %copy-start.38 = (bf16[128,4096]{1,0:T(8,128)(2,1)S(1)}, bf16[128,4096]{1,0:T(8,128)(2,1)}, u32[]{:S(2)}) copy-start(bf16[128,4096]{1,0:T(8,128)(2,1)} %param.27) | copy-start | bytes 3145732
  283.7 11.8 %all-to-all-start.5 = ((f32[16,1,512]{2,1,0:T(1,128)}), f32[16,1,512]{2,1,0:T(1,128)S(1)}, u32[]{:S(2)}, u32[]{:S(2)}) async-start(f32[16,1,512]{2,1,0:T(1,128)} %broadcast_in_dim.94), calls=%async_computation.6 | async-start | bytes 65536 | tf_op jit(solution)/shard_map/all_to_all | solution.py:11
  291.5 23.9 %copy-start.5 = (bf16[256,128]{1,0:T(8,128)(2,1)S(1)}, bf16[256,128]{1,0:T(8,128)(2,1)}, u32[]{:S(2)}) copy-start(bf16[256,128]{1,0:T(8,128)(2,1)} %param.23) | copy-start | bytes 196612
  291.5 23.9 %copy-start.6 = (bf16[256,128]{1,0:T(8,128)(2,1)S(1)}, bf16[256,128]{1,0:T(8,128)(2,1)}, u32[]{:S(2)}) copy-start(bf16[256,128]{1,0:T(8,128)(2,1)} %param.22) | copy-start | bytes 196612
  291.5 23.9 %copy-start.11 = (f32[128]{0:T(128)S(1)}, f32[128]{0:T(128)}, u32[]{:S(2)}) copy-start(f32[128]{0:T(128)} %get-tuple-element.66) | copy-start | bytes 1540
  291.5 23.9 %copy-start.12 = (f32[128]{0:T(128)S(1)}, f32[128]{0:T(128)}, u32[]{:S(2)}) copy-start(f32[128]{0:T(128)} %get-tuple-element.67) | copy-start | bytes 1540
  291.5 23.9 %copy-start.13 = (f32[128]{0:T(128)S(1)}, f32[128]{0:T(128)}, u32[]{:S(2)}) copy-start(f32[128]{0:T(128)} %get-tuple-element.68) | copy-start | bytes 1540
  291.5 23.9 %copy-start.14 = (f32[128]{0:T(128)S(1)}, f32[128]{0:T(128)}, u32[]{:S(2)}) copy-start(f32[128]{0:T(128)} %get-tuple-element.69) | copy-start | bytes 1540
  291.5 23.9 %copy-start.15 = (f32[128]{0:T(128)S(1)}, f32[128]{0:T(128)}, u32[]{:S(2)}) copy-start(f32[128]{0:T(128)} %get-tuple-element.70) | copy-start | bytes 1540
  291.6 23.9 %copy-start.16 = (f32[128]{0:T(128)S(1)}, f32[128]{0:T(128)}, u32[]{:S(2)}) copy-start(f32[128]{0:T(128)} %get-tuple-element.40) | copy-start | bytes 1540
  291.6 23.9 %copy-start.17 = (f32[128]{0:T(128)S(1)}, f32[128]{0:T(128)}, u32[]{:S(2)}) copy-start(f32[128]{0:T(128)} %get-tuple-element.41) | copy-start | bytes 1540
  291.6 23.9 %copy-start.18 = (f32[128]{0:T(128)S(1)}, f32[128]{0:T(128)}, u32[]{:S(2)}) copy-start(f32[128]{0:T(128)} %get-tuple-element.42) | copy-start | bytes 1540
  291.6 23.9 %copy-start.19 = (f32[128]{0:T(128)S(1)}, f32[128]{0:T(128)}, u32[]{:S(2)}) copy-start(f32[128]{0:T(128)} %get-tuple-element.43) | copy-start | bytes 1540
  291.6 23.9 %copy-start.20 = (f32[128]{0:T(128)S(1)}, f32[128]{0:T(128)}, u32[]{:S(2)}) copy-start(f32[128]{0:T(128)} %get-tuple-element.44) | copy-start | bytes 1540
  291.6 23.9 %copy-start.21 = (f32[128]{0:T(128)S(1)}, f32[128]{0:T(128)}, u32[]{:S(2)}) copy-start(f32[128]{0:T(128)} %get-tuple-element.45) | copy-start | bytes 1540
  291.6 23.9 %copy-start.22 = (f32[128]{0:T(128)S(1)}, f32[128]{0:T(128)}, u32[]{:S(2)}) copy-start(f32[128]{0:T(128)} %get-tuple-element.46) | copy-start | bytes 1540
  291.6 23.9 %copy-start.23 = (f32[128]{0:T(128)S(1)}, f32[128]{0:T(128)}, u32[]{:S(2)}) copy-start(f32[128]{0:T(128)} %get-tuple-element.47) | copy-start | bytes 1540
  291.6 23.9 %copy-start.24 = (f32[128]{0:T(128)S(1)}, f32[128]{0:T(128)}, u32[]{:S(2)}) copy-start(f32[128]{0:T(128)} %get-tuple-element.48) | copy-start | bytes 1540
  291.6 23.9 %copy-start.25 = (f32[128]{0:T(128)S(1)}, f32[128]{0:T(128)}, u32[]{:S(2)}) copy-start(f32[128]{0:T(128)} %get-tuple-element.49) | copy-start | bytes 1540
  291.7 23.9 %copy-start.26 = (f32[128]{0:T(128)S(1)}, f32[128]{0:T(128)}, u32[]{:S(2)}) copy-start(f32[128]{0:T(128)} %get-tuple-element.50) | copy-start | bytes 1540
  291.7 23.9 %copy-start.27 = (f32[128]{0:T(128)S(1)}, f32[128]{0:T(128)}, u32[]{:S(2)}) copy-start(f32[128]{0:T(128)} %get-tuple-element.51) | copy-start | bytes 1540
  291.7 23.9 %copy-start.28 = (f32[128]{0:T(128)S(1)}, f32[128]{0:T(128)}, u32[]{:S(2)}) copy-start(f32[128]{0:T(128)} %get-tuple-element.52) | copy-start | bytes 1540
  291.7 23.9 %copy-start.29 = (f32[128]{0:T(128)S(1)}, f32[128]{0:T(128)}, u32[]{:S(2)}) copy-start(f32[128]{0:T(128)} %get-tuple-element.53) | copy-start | bytes 1540
  291.7 23.9 %copy-start.30 = (f32[128]{0:T(128)S(1)}, f32[128]{0:T(128)}, u32[]{:S(2)}) copy-start(f32[128]{0:T(128)} %get-tuple-element.54) | copy-start | bytes 1540
  291.7 23.9 %copy-start.31 = (f32[128]{0:T(128)S(1)}, f32[128]{0:T(128)}, u32[]{:S(2)}) copy-start(f32[128]{0:T(128)} %get-tuple-element.55) | copy-start | bytes 1540
  291.7 23.9 %copy-start.32 = (f32[128]{0:T(128)S(1)}, f32[128]{0:T(128)}, u32[]{:S(2)}) copy-start(f32[128]{0:T(128)} %get-tuple-element.56) | copy-start | bytes 1540
  291.7 23.9 %copy-start.33 = (f32[128]{0:T(128)S(1)}, f32[128]{0:T(128)}, u32[]{:S(2)}) copy-start(f32[128]{0:T(128)} %get-tuple-element.57) | copy-start | bytes 1540
  291.7 23.9 %copy-start.34 = (f32[128]{0:T(128)S(1)}, f32[128]{0:T(128)}, u32[]{:S(2)}) copy-start(f32[128]{0:T(128)} %get-tuple-element.58) | copy-start | bytes 1540
  295.5 22.9 %all-to-all-start.4 = ((bf16[16,256,128]{2,1,0:T(8,128)(2,1)}), bf16[16,256,128]{2,1,0:T(8,128)(2,1)S(1)}, u32[]{:S(2)}, u32[]{:S(2)}) async-start(bf16[16,256,128]{2,1,0:T(8,128)(2,1)} %bitcast.17), calls=%async_computation.5 | async-start | bytes 2097152 | tf_op jit(solution)/shard_map/all_to_all | solution.py:58
  302.3 13.1 %collective-permute-start = (f32[30,128]{1,0:T(8,128)S(1)}, f32[30,128]{1,0:T(8,128)S(1)}, u32[]{:S(2)}, u32[]{:S(2)}) collective-permute-start(f32[30,128]{1,0:T(8,128)S(1)} %slice.309), channel_id=1, source_target_pairs={{16,0},{32,16},{48,32},{64,48},{80,64},{96,80},{112,96},{128,112},... | collective-permute-start | bytes 46088 | tf_op jit(solution)/shard_map/ppermute | solution.py:65
Sparse Core Ops, SparseCore 0:
  55.0 79.9 all-gather.2
  153.1 61.6 reduce-scatter.1
  248.5 32.0 all-gather.4
where the time goes:
time: 327 us; the launch traced here: 326 us
  waiting for transfers between devices  179 us (55%)
  matrix products  41.5 us (13%)
  blocking collectives  35.4 us (11%)
  starting transfers between devices  32.3 us (10%)
  between operations  14.4 us (4%)
  local copies, waits for them, and re-layouts  14 us (4%)
  other arithmetic  9.31 us (3%)
    all_gather x1, waiting for transfers between devices, in_one_piece(): out = lax.all_gather(both, axis, axis=dim, tiled=True)  79.9 us
    reduce_scatter x1, waiting for transfers between devices, per_device(): lax.psum_scatter(input_part.astype(jnp.bfloat16), 'tp', scatter_dimension...  61.9 us
    all_to_all x3, starting transfers between devices, sent_to_all(): lax.all_to_all(jnp.broadcast_to(value[None], (count, *value.shape)), axis...  23.9 us
    all_to_all x1, blocking collectives, side_by_side(): lax.all_to_all(both, axis, split_axis=split_dim, concat_axis=concat_dim,...  20.6 us
    all_gather x1, waiting for transfers between devices, per_device(): full_grad = lax.all_gather(stream_grad, 'tp', axis=1, tiled=True)  18.9 us
    all_to_all x1, blocking collectives, per_device(): lax.all_to_all(input_back.reshape(token_groups, capacity, width_part), 's...  14.7 us
    all_to_all x3, waiting for transfers between devices, sent_to_all(): lax.all_to_all(jnp.broadcast_to(value[None], (count, *value.shape)), axis...  10.7 us
    ppermute x1, waiting for transfers between devices, shifted(): return lax.ppermute(block, axis, route)  6.6 us
  transfers between devices with their start and end apart: 8, of which 7 were waited for; matrix products, arithmetic and copies ran while one was open for 10% of the time, Pallas kernels for 0%

commit v1 on v0

--- a/solution.py
+++ b/solution.py
@@ -190,7 +190,16 @@
     inner_sum = of_everyone(jnp.sum(gained * residual, axis=1), "tp")
     norm_back = inverse * gained - residual * inverse**3 * (inner_sum / model_width)[:, None]
     stream_grad = (upstream.astype(jnp.float32) + norm_back).astype(jnp.bfloat16)
-    full_grad = lax.all_gather(stream_grad, "tp", axis=1, tiled=True)
+    list_rates = lambda matrix, shard_axis: jnp.concatenate(
+        lax.all_to_all(
+            jnp.stack(lax.axis_size(shard_axis) * [matrix], 0),
+            shard_axis,
+            split_axis=0,
+            concat_axis=0,
+        ),
+        1,
+    )
+    full_grad = list_rates(stream_grad, "tp")
     mean_val = (conv_total / channels)[:, None]
     variance = (conv_squares / channels)[:, None] - mean_val * mean_val
     inv_std = lax.rsqrt(variance + EPSILON)

time: 327 us -> 346 us (1.058)
  waiting for transfers between devices: 179 us -> 200 us
    all_to_all x0 -> x1, waiting for transfers between devices: none -> 37.2 us  [per_device(): lax.all_to_all(jnp.stack(lax.axis_size(shard_axis) * [matrix], 0), shard_...]
    all_gather x1 -> x0, waiting for transfers between devices: 18.9 us -> none  [per_device(): full_grad = lax.all_gather(stream_grad, 'tp', axis=1, tiled=True)]
    all_to_all x0 -> x1, starting transfers between devices: none -> 3.9 us  [per_device(): lax.all_to_all(jnp.stack(lax.axis_size(shard_axis) * [matrix], 0), shard_...]
  transfers between devices with their start and end apart: 8 -> 8, of which waited for: 7 -> 7; matrix products, arithmetic and copies ran while one was open for 10% -> 9% of each run, Pallas kernels for 0% -> 0%
where the time goes in v1:
time: 346 us; the launch traced here: 345 us
  waiting for transfers between devices  200 us (58%)
  matrix products  39.8 us (12%)
  blocking collectives  35.2 us (10%)
  starting transfers between devices  33.5 us (10%)
  between operations  14.4 us (4%)
  local copies, waits for them, and re-layouts  14.2 us (4%)
  other arithmetic  8.03 us (2%)
    all_gather x1, waiting for transfers between devices, in_one_piece(): out = lax.all_gather(both, axis, axis=dim, tiled=True)  79.9 us
    reduce_scatter x1, waiting for transfers between devices, per_device(): lax.psum_scatter(input_part.astype(jnp.bfloat16), 'tp', scatter_dimension...  62 us
    all_to_all x1, waiting for transfers between devices, per_device(): lax.all_to_all(jnp.stack(lax.axis_size(shard_axis) * [matrix], 0), shard_...  37.2 us
    all_to_all x3, starting transfers between devices, sent_to_all(): lax.all_to_all(jnp.broadcast_to(value[None], (count, *value.shape)), axis...  24.4 us
    all_to_all x1, blocking collectives, side_by_side(): lax.all_to_all(both, axis, split_axis=split_dim, concat_axis=concat_dim,...  20.6 us
    all_to_all x1, blocking collectives, per_device(): lax.all_to_all(input_back.reshape(token_groups, capacity, width_part), 's...  14.6 us
    all_to_all x3, waiting for transfers between devices, sent_to_all(): lax.all_to_all(jnp.broadcast_to(value[None], (count, *value.shape)), axis...  12.7 us
  transfers between devices with their start and end apart: 8, of which 7 were waited for; matrix products, arithmetic and copies ran while one was open for 9% of the time, Pallas kernels for 0%

profile of v1, /device:TPU:1, one launch (start us, length us, event | category | flops | bytes accessed | tf_op | source)
XLA Modules:
  0.0 345.0 jit_solution(11315314069520617895)
XLA Ops:
  7.2 1.1 copy.70
  8.3 1.0 convert_reduce_fusion.1
  9.3 0.1 fusion.29
  9.3 0.6 broadcast_in_dim.81
  10.0 10.0 %all-to-all-start = ((f32[16,1,768]{2,1,0:T(1,128)}), f32[16,1,768]{2,1,0:T(1,128)S(1)}, u32[]{:S(2)}, u32[]{:S(2)}) async-start(f32[16,1,768]{2,1,0:T(1,128)} %broadcast_in_dim.81), calls=%async_computation | async-start | bytes 98304 | tf_op jit(solution)/shard_map/all_to_all | solution.py:11
  20.0 0.8 copy.72
  20.8 0.1 eq.56
  21.0 0.1 eq.60
  21.1 1.2 reduce-window.6
  22.3 0.2 slice_reduce_fusion
  22.5 0.1 fusion.149
  22.6 0.1 reduce_sum.124
  22.8 0.1 copy.75
  22.9 0.7 multiply_add_fusion
  23.6 0.2 fusion.23
  23.8 0.2 select_reduce_fusion
  24.0 0.8 fusion.157
  24.8 0.2 add_reduce_fusion
  25.0 0.1 mul.484
  25.1 0.9 concatenate.23
  26.0 2.7 gather_fusion.1
  28.7 0.2 fusion.20
  29.0 0.8 fusion.28
  29.7 0.1 copy.89
  29.9 2.7 gather_fusion
  32.5 0.1 pad_maximum_fusion
  32.6 20.6 %all_to_all.38 = bf16[16,96,256]{2,1,0:T(8,128)(2,1)S(1)} all-to-all(bf16[16,96,256]{2,1,0:T(8,128)(2,1)S(1)} %pad_maximum_fusion), channel_id=1, replica_groups=mesh['sp'=16,'tp'=16] {'sp'}, dimensions={0} | all-to-all | bytes 1572864 | tf_op jit(solution)/shard_map/all_to_all | solution.py:33
  53.2 0.1 fusion.156
  53.3 0.9 pad_maximum_fusion.1
  54.3 0.2 reduce-scatter.2.cloned.1.call-start
  54.5 79.9 %all-gather.2.cloned.1.call-done = bf16[1536,4096]{1,0:T(8,128)(2,1)} async-done(((bf16[1536,256]{1,0:T(8,128)(2,1)}), bf16[1536,4096]{1,0:T(8,128)(2,1)}) %all-gather.2.cloned.1.call-update) | async-done | bytes 12582928 | tf_op jit(solution)/shard_map/all_gather | solution.py:46
  134.3 4.7 %fusion.9 = f32[768,128]{1,0:T(8,128)S(1)} fusion(bf16[1536,4096]{1,0:T(8,128)(2,1)} %all-gather.2.cloned.1.call-done, bf16[1,4096,128]{2,1,0:T(8,128)(2,1)S(1)} %copy-done), kind=kOutput, calls=%fused_computation.13 | convolution fusion | flops 805306368 | bytes 7733248 | tf_op jit(solution)/shard_map/dot_general | solution.py:153
  139.1 5.4 %fusion.11 = f32[768,128]{1,0:T(8,128)S(1)} fusion(bf16[1536,4096]{1,0:T(8,128)(2,1)} %all-gather.2.cloned.1.call-done, bf16[1,4096,128]{2,1,0:T(8,128)(2,1)S(1)} %copy-done.2), kind=kOutput, calls=%fused_computation.15 | convolution fusion | flops 805306368 | bytes 7733248 | tf_op jit(solution)/shard_map/dot_general | solution.py:154
  144.5 1.8 multiply_convert_fusion.1
  146.3 1.8 fusion.14
  148.1 4.5 %add_convert_fusion = bf16[768,4096]{1,0:T(8,128)(2,1)} fusion(f32[768,4096]{1,0:T(8,128)S(1)} %fusion.14, bf16[768,128]{1,0:T(8,128)(2,1)S(1)} %get-tuple-element.36, bf16[1,4096,128]{2,1,0:T(8,128)(2,1)S(1)} %copy-done.2), kind=kOutput, calls=%fused_computation.2 | convolution fusion | flops 811597824 | bytes 20119552 | tf_op jit(solution)/shard_map/dot_general | solution.py:172
  152.6 62.0 %reduce-scatter.2.cloned.1.call-done = bf16[768,256]{1,0:T(8,128)(2,1)} async-done(((bf16[768,4096]{1,0:T(8,128)(2,1)}), bf16[768,256]{1,0:T(8,128)(2,1)}) %reduce-scatter.2.cloned.1.call-update) | async-done | bytes 393232 | tf_op jit(solution)/shard_map/reduce_scatter | solution.py:175
  214.7 14.6 %all_to_all.39 = bf16[16,48,256]{2,1,0:T(8,128)(2,1)S(1)} all-to-all(bf16[16,48,256]{2,1,0:T(8,128)(2,1)} %bitcast.134), channel_id=1, replica_groups=mesh['sp'=16,'tp'=16] {'sp'}, dimensions={0} | all-to-all | bytes 786432 | tf_op jit(solution)/shard_map/all_to_all | solution.py:178
  229.3 0.4 fusion.34
  229.7 0.6 broadcast_in_dim.93
  230.3 9.6 %all-to-all-start.3 = ((f32[16,1,256]{2,1,0:T(1,128)}), f32[16,1,256]{2,1,0:T(1,128)S(1)}, u32[]{:S(2)}, u32[]{:S(2)}) async-start(f32[16,1,256]{2,1,0:T(1,128)} %broadcast_in_dim.93), calls=%async_computation.4 | async-start | bytes 32768 | tf_op jit(solution)/shard_map/all_to_all | solution.py:11
  239.9 0.1 copy.77
  240.0 7.2 %all-to-all-done.3 = f32[16,1,256]{2,1,0:T(1,128)S(1)} async-done(((f32[16,1,256]{2,1,0:T(1,128)}), f32[16,1,256]{2,1,0:T(1,128)S(1)}, u32[]{:S(2)}, u32[]{:S(2)}) %all-to-all-start.3) | async-done | bytes 16416 | tf_op jit(solution)/shard_map/all_to_all | solution.py:11
  247.3 0.1 fusion.33
  247.3 1.5 stack.2
  248.9 3.9 %all-to-all-start.4 = ((bf16[16,256,256]{1,2,0:T(8,128)(2,1)}), bf16[16,256,256]{1,2,0:T(8,128)(2,1)S(1)}, u32[]{:S(2)}, u32[]{:S(2)}) async-start(bf16[16,256,256]{1,2,0:T(8,128)(2,1)} %stack.2), calls=%async_computation.5 | async-start | bytes 4194304 | tf_op jit(solution)/shard_map/all_to_all | solution.py:194
  252.8 5.9 %convolution_bitcast_fusion.1 = f32[1,4096,128]{2,1,0:T(8,128)} fusion(bf16[768,128]{1,0:T(8,128)(2,1)} %copy-done.8, bf16[1536,4096]{1,0:T(8,128)(2,1)} %all-gather.2.cloned.1.call-done), kind=kOutput, calls=%fused_computation.9 | convolution fusion | flops 805306368 | bytes 8585216 | tf_op jit(solution)/shard_map/dot_general | solution.py:161
  258.8 6.0 %convolution_bitcast_fusion = f32[1,4096,128]{2,1,0:T(8,128)} fusion(bf16[768,128]{1,0:T(8,128)(2,1)S(1)} %get-tuple-element.36, bf16[1536,4096]{1,0:T(8,128)(2,1)} %all-gather.2.cloned.1.call-done), kind=kOutput, calls=%fused_computation.8 | convolution fusion | flops 805306368 | bytes 8585216 | tf_op jit(solution)/shard_map/dot_general | solution.py:164
  264.7 37.2 %all-to-all-done.4 = bf16[16,256,256]{1,2,0:T(8,128)(2,1)S(1)} async-done(((bf16[16,256,256]{1,2,0:T(8,128)(2,1)}), bf16[16,256,256]{1,2,0:T(8,128)(2,1)S(1)}, u32[]{:S(2)}, u32[]{:S(2)}) %all-to-all-start.4) | async-done | bytes 2097184 | tf_op jit(solution)/shard_map/all_to_all | solution.py:194
  301.9 2.1 fusion.154
  304.0 0.6 broadcast_in_dim.94
  304.6 4.8 %all-to-all-start.6 = ((f32[16,1,512]{2,1,0:T(1,128)}), f32[16,1,512]{2,1,0:T(1,128)S(1)}, u32[]{:S(2)}, u32[]{:S(2)}) async-start(f32[16,1,512]{2,1,0:T(1,128)} %broadcast_in_dim.94), calls=%async_computation.7 | async-start | bytes 65536 | tf_op jit(solution)/shard_map/all_to_all | solution.py:11
  309.5 1.9 convolution_convert_fusion
  311.3 5.5 %all-to-all-done.6 = f32[16,1,512]{2,1,0:T(1,128)S(1)} async-done(((f32[16,1,512]{2,1,0:T(1,128)}), f32[16,1,512]{2,1,0:T(1,128)S(1)}, u32[]{:S(2)}, u32[]{:S(2)}) %all-to-all-start.6) | async-done | bytes 32800 | tf_op jit(solution)/shard_map/all_to_all | solution.py:11
  316.8 3.7 %all-to-all-start.5 = ((bf16[16,256,128]{2,1,0:T(8,128)(2,1)}), bf16[16,256,128]{2,1,0:T(8,128)(2,1)S(1)}, u32[]{:S(2)}, u32[]{:S(2)}) async-start(bf16[16,256,128]{2,1,0:T(8,128)(2,1)} %bitcast.128), calls=%async_computation.6 | async-start | bytes 2097152 | tf_op jit(solution)/shard_map/all_to_all | solution.py:58
  320.6 0.2 fusion.139
  320.8 1.3 collective-permute-start
  322.1 5.4 %fusion.4 = f32[1,128,4096]{2,1,0:T(8,128)} fusion(bf16[1536,4096]{1,0:T(8,128)(2,1)} %all-gather.2.cloned.1.call-done, f32[768,128]{1,0:T(8,128)} %copy-done.6, f32[768,128]{1,0:T(8,128)} %copy-done.5), kind=kOutput, calls=%fused_computation.7 | convolution fusion | flops 805896192 | bytes 9175040 | tf_op jit(solution)/shard_map/dot_general | solution.py:167
  327.5 6.5 %collective-permute-done = f32[30,128]{1,0:T(8,128)S(1)} collective-permute-done((f32[30,128]{1,0:T(8,128)S(1)}, f32[30,128]{1,0:T(8,128)S(1)}, u32[]{:S(2)}, u32[]{:S(2)}) %collective-permute-start) | collective-permute-done | bytes 15392 | tf_op jit(solution)/shard_map/ppermute | solution.py:65
  334.0 1.1 multiply_convert_fusion.4
  335.1 0.7 multiply_convert_fusion.5
  335.8 1.5 all-to-all-done.5
  337.3 0.1 convert_reduce_fusion
  337.4 0.8 copy.80
  (51 shorter events, 0.4 us)
Async XLA Ops:
  7.2 127.2 %copy-start = (bf16[1,4096,128]{2,1,0:T(8,128)(2,1)S(1)}, bf16[1,4096,128]{2,1,0:T(8,128)(2,1)}, u32[]{:S(2)}) copy-start(bf16[1,4096,128]{2,1,0:T(8,128)(2,1)} %param.19) | copy-start | bytes 3145732
  10.0 18.9 %all-to-all-start = ((f32[16,1,768]{2,1,0:T(1,128)}), f32[16,1,768]{2,1,0:T(1,128)S(1)}, u32[]{:S(2)}, u32[]{:S(2)}) async-start(f32[16,1,768]{2,1,0:T(1,128)} %broadcast_in_dim.81), calls=%async_computation | async-start | bytes 98304 | tf_op jit(solution)/shard_map/all_to_all | solution.py:11
  20.0 114.4 %all-gather.2.cloned.1.call-start = ((), (), s32[]{:S(2)}) async-start(), calls=%async_computation.8 | async-start | bytes 13369344 | tf_op jit(solution)/shard_map/all_gather | solution.py:46
  53.3 85.8 %copy-start.2 = (bf16[1,4096,128]{2,1,0:T(8,128)(2,1)S(1)}, bf16[1,4096,128]{2,1,0:T(8,128)(2,1)}, u32[]{:S(2)}) copy-start(bf16[1,4096,128]{2,1,0:T(8,128)(2,1)} %param.20) | copy-start | bytes 3145732
  54.3 160.4 %reduce-scatter.2.cloned.1.call-start = ((), (), s32[]{:S(2)}) async-start(), calls=%async_computation.9 | async-start | bytes 6684672 | tf_op jit(solution)/shard_map/reduce_scatter | solution.py:175
  134.3 10.1 %copy-start.1 = (bf16[1536,4096]{1,0:T(8,128)(2,1)S(1)}, bf16[1536,4096]{1,0:T(8,128)(2,1)}, u32[]{:S(2)}) copy-start(bf16[1536,4096]{1,0:T(8,128)(2,1)} %all-gather.2.cloned.1.call-done) | copy-start | bytes 37748740
  139.1 9.1 %copy-start.5 = (f32[768,128]{1,0:T(8,128)}, f32[768,128]{1,0:T(8,128)S(1)}, u32[]{:S(2)}) copy-start(f32[768,128]{1,0:T(8,128)S(1)} %fusion.9) | copy-start | bytes 1179652
  139.1 5.4 %copy-start.13 = (bf16[1,128,4096]{2,1,0:T(8,128)(2,1)S(1)}, bf16[1,128,4096]{2,1,0:T(8,128)(2,1)}, u32[]{:S(2)}) copy-start(bf16[1,128,4096]{2,1,0:T(8,128)(2,1)} %param.21) | copy-start | bytes 3145732
  144.5 1.8 copy-start.6
  146.3 1.8 copy-start.8
  152.6 76.7 %copy-start.11 = (f32[256]{0:T(256)S(1)}, f32[256]{0:T(256)}, u32[]{:S(2)}) copy-start(f32[256]{0:T(256)} %param.16) | copy-start | bytes 3076
  152.6 87.3 %copy-start.4 = (bf16[256,256]{1,0:T(8,128)(2,1)S(1)}, bf16[256,256]{1,0:T(8,128)(2,1)}, u32[]{:S(2)}) copy-start(bf16[256,256]{1,0:T(8,128)(2,1)} %param.14) | copy-start | bytes 393220
  152.6 100.1 %copy-start.10 = (f32[31,128]{1,0:T(8,128)S(1)}, f32[31,128]{1,0:T(8,128)}, u32[]{:S(2)}) copy-start(f32[31,128]{1,0:T(8,128)} %param.26) | copy-start | bytes 47620
  230.3 16.9 %all-to-all-start.3 = ((f32[16,1,256]{2,1,0:T(1,128)}), f32[16,1,256]{2,1,0:T(1,128)S(1)}, u32[]{:S(2)}, u32[]{:S(2)}) async-start(f32[16,1,256]{2,1,0:T(1,128)} %broadcast_in_dim.93), calls=%async_computation.4 | async-start | bytes 32768 | tf_op jit(solution)/shard_map/all_to_all | solution.py:11
  248.9 53.0 %all-to-all-start.4 = ((bf16[16,256,256]{1,2,0:T(8,128)(2,1)}), bf16[16,256,256]{1,2,0:T(8,128)(2,1)S(1)}, u32[]{:S(2)}, u32[]{:S(2)}) async-start(bf16[16,256,256]{1,2,0:T(8,128)(2,1)} %stack.2), calls=%async_computation.5 | async-start | bytes 4194304 | tf_op jit(solution)/shard_map/all_to_all | solution.py:194
  258.8 43.1 %copy-start.3 = (bf16[256,128]{1,0:T(8,128)(2,1)S(1)}, bf16[256,128]{1,0:T(8,128)(2,1)}, u32[]{:S(2)}) copy-start(bf16[256,128]{1,0:T(8,128)(2,1)} %param.24) | copy-start | bytes 196612
  258.8 43.1 %copy-start.12 = (f32[128]{0:T(128)S(1)}, f32[128]{0:T(128)}, u32[]{:S(2)}) copy-start(f32[128]{0:T(128)} %param.25) | copy-start | bytes 1540
  304.6 12.2 %all-to-all-start.6 = ((f32[16,1,512]{2,1,0:T(1,128)}), f32[16,1,512]{2,1,0:T(1,128)S(1)}, u32[]{:S(2)}, u32[]{:S(2)}) async-start(f32[16,1,512]{2,1,0:T(1,128)} %broadcast_in_dim.94), calls=%async_computation.7 | async-start | bytes 65536 | tf_op jit(solution)/shard_map/all_to_all | solution.py:11
  311.3 22.7 %copy-start.7 = (bf16[256,128]{1,0:T(8,128)(2,1)S(1)}, bf16[256,128]{1,0:T(8,128)(2,1)}, u32[]{:S(2)}) copy-start(bf16[256,128]{1,0:T(8,128)(2,1)} %param.23) | copy-start | bytes 196612
  311.3 22.7 %copy-start.9 = (bf16[256,128]{1,0:T(8,128)(2,1)S(1)}, bf16[256,128]{1,0:T(8,128)(2,1)}, u32[]{:S(2)}) copy-start(bf16[256,128]{1,0:T(8,128)(2,1)} %param.22) | copy-start | bytes 196612
  316.8 20.5 %all-to-all-start.5 = ((bf16[16,256,128]{2,1,0:T(8,128)(2,1)}), bf16[16,256,128]{2,1,0:T(8,128)(2,1)S(1)}, u32[]{:S(2)}, u32[]{:S(2)}) async-start(bf16[16,256,128]{2,1,0:T(8,128)(2,1)} %bitcast.128), calls=%async_computation.6 | async-start | bytes 2097152 | tf_op jit(solution)/shard_map/all_to_all | solution.py:58
  320.8 13.2 %collective-permute-start = (f32[30,128]{1,0:T(8,128)S(1)}, f32[30,128]{1,0:T(8,128)S(1)}, u32[]{:S(2)}, u32[]{:S(2)}) collective-permute-start(f32[30,128]{1,0:T(8,128)S(1)} %slice.309), channel_id=1, source_target_pairs={{16,0},{32,16},{48,32},{64,48},{80,64},{96,80},{112,96},{128,112},... | collective-permute-start | bytes 46088 | tf_op jit(solution)/shard_map/ppermute | solution.py:65
Sparse Core Ops, SparseCore 0:
  54.4 79.9 all-gather.1
  152.8 61.8 reduce-scatter.1
